TPU v7x, 32 devices: a whole 2x2x4 slice. The times are simulated.
32 devices in a mesh: sp: 8 (over z, y), dp: 4 (over x, core).
Axes of the slice: x: 2, y: 2, z: 4, core: 2. Of those that a mesh axis runs over, the one named last changes fastest.
Arguments:
- tokens: bfloat16 [4, 1024, 2048], P('dp', 'sp'), may hold values from -6 to 6
- cotangent: bfloat16 [4, 1024, 2048], P('dp', 'sp'), may hold values from -6 to 6
- value_weight: bfloat16 [2048, 2048], P(('sp', 'dp')), may hold values from -0.125 to 0.125
- query_heads: bfloat16 [4, 1024, 16, 128], P('dp', None, 'sp'), may hold values from -8 to 8
- key_heads: bfloat16 [4, 1024, 16, 128], P('dp', None, 'sp'), may hold values from -8 to 8
- lambdas: float32 [16], P('sp'), may hold values from 0.3 to 0.8
Outputs:
- grad_query: bfloat16 [4, 1024, 16, 128], P('dp', None, 'sp')
- grad_key: bfloat16 [4, 1024, 16, 128], P('dp', None, 'sp')
- grad_tokens: bfloat16 [4, 1024, 2048], P('dp', 'sp')
- grad_value_weight: float32 [2048, 2048], P(('sp', 'dp'))
- grad_lambda: float32 [16], P('sp')
All inputs are finite; a program needn't handle non-finite values.
Results may differ from a plain program's by a relative error of at most 0.0095.
Values may be sent and summed in bfloat16 or wider, within the bound.
No kernel may reach another device: no remote copies, remote signals or barrier semaphores. Data moves between devices by JAX's collectives and lax.ppermute only.
A program may use at most 192 MiB of HBM per device.

v0:
```python
import jax
import jax.numpy as jnp
from jax import lax
from jax.sharding import PartitionSpec as P

QBLOCK = 256


EPS = 1e-06
NEGATIVE = -1e30


def head_backward(queries, keys_in, values_in, cotangent, lambdas, block_rows):
    seq_length = queries.shape[0]
    head_count = queries.shape[1]
    head_width = queries.shape[3]
    scaling = head_width ** (-0.5)
    blocks_count = seq_length // block_rows
    lambda_col = lambdas[:, None, None]
    grad_key_sum = jnp.zeros(keys_in.shape, jnp.float32)
    grad_value_sum = jnp.zeros(values_in.shape, jnp.float32)
    grad_lambda_sum = jnp.zeros((head_count,), jnp.float32)
    query_blocks = []
    for block_index in range(blocks_count):
        offset = block_index * block_rows
        reach = offset + block_rows
        query_block = queries[offset:reach]
        cotan_block = cotangent[offset:reach].astype(jnp.float32)
        keys_seen = keys_in[:reach]
        values_seen = values_in[:reach]
        scores = (
            jnp.einsum(
                "qhcd,khcd->hcqk", query_block, keys_seen, preferred_element_type=jnp.float32
            )
            * scaling
        )
        rows_pos = offset + jnp.arange(block_rows, dtype=jnp.int32)
        allowed = rows_pos[:, None] >= jnp.arange(reach, dtype=jnp.int32)[None, :]
        scores = jnp.where(allowed, scores, NEGATIVE)
        highest = jnp.max(scores, axis=-1, keepdims=True)
        exponent = jnp.exp(scores - highest)
        softmaxes = exponent / jnp.sum(exponent, axis=-1, keepdims=True)
        weights = (softmaxes[:, 0] - lambda_col * softmaxes[:, 1]).astype(jnp.bfloat16)
        mixed_out = jnp.einsum(
            "hqk,khd->qhd", weights, values_seen, preferred_element_type=jnp.float32
        )
        inverse = lax.rsqrt(jnp.mean(mixed_out * mixed_out, axis=-1, keepdims=True) + EPS)
        normed = mixed_out * inverse
        grad_mixed = (
            inverse
            * (cotan_block - normed * jnp.mean(cotan_block * normed, axis=-1, keepdims=True))
        ).astype(jnp.bfloat16)
        grad_weights = jnp.einsum(
            "qhd,khd->hqk", grad_mixed, values_seen, preferred_element_type=jnp.float32
        )
        value_part = jnp.einsum(
            "hqk,qhd->khd", weights, grad_mixed, preferred_element_type=jnp.float32
        )
        grad_value_sum = grad_value_sum.at[:reach].add(value_part)
        grad_lambda_sum = grad_lambda_sum - jnp.sum(grad_weights * softmaxes[:, 1], axis=(1, 2))
        first_grad = softmaxes[:, 0] * (
            grad_weights - jnp.sum(grad_weights * softmaxes[:, 0], axis=-1, keepdims=True)
        )
        second_grad = (
            -lambda_col
            * softmaxes[:, 1]
            * (grad_weights - jnp.sum(grad_weights * softmaxes[:, 1], axis=-1, keepdims=True))
        )
        grad_scores = (jnp.stack([first_grad, second_grad], axis=1) * scaling).astype(jnp.bfloat16)
        query_blocks.append(
            jnp.einsum(
                "hcqk,khcd->qhcd", grad_scores, keys_seen, preferred_element_type=jnp.float32
            ).astype(jnp.bfloat16)
        )
        key_part = jnp.einsum(
            "hcqk,qhcd->khcd", grad_scores, query_block, preferred_element_type=jnp.float32
        )
        grad_key_sum = grad_key_sum.at[:reach].add(key_part)
    grad_query = jnp.concatenate(query_blocks, axis=0)
    return (
        grad_query,
        grad_key_sum.astype(jnp.bfloat16),
        grad_value_sum.astype(jnp.bfloat16),
        grad_lambda_sum,
    )


def body(tokens, cotangent, value_weight, query_heads, key_heads, lambdas):
    local_tokens = tokens[0]
    row_count = value_weight.shape[0]
    value_rows = jnp.dot(
        local_tokens,
        lax.all_gather(value_weight, ("sp", "dp"), axis=0, tiled=True),
        preferred_element_type=jnp.float32,
    )
    value_tokens = value_rows.astype(jnp.bfloat16)[None]
    cotan_heads, value_heads = (
        lax.all_to_all(cotangent, "sp", split_axis=2, concat_axis=1, tiled=True),
        lax.all_to_all(value_tokens, "sp", split_axis=2, concat_axis=1, tiled=True),
    )
    seq_length = cotan_heads.shape[1]
    head_count = query_heads.shape[2]
    head_width = query_heads.shape[3] // 2
    queries = query_heads[0].reshape(seq_length, head_count, 2, head_width)
    keys_in = key_heads[0].reshape(seq_length, head_count, 2, head_width)
    values_in = value_heads[0].reshape(seq_length, head_count, 2 * head_width)
    cotan_in = cotan_heads[0].reshape(seq_length, head_count, 2 * head_width)
    grad_query, grad_key, grad_value, grad_lambda = head_backward(
        queries, keys_in, values_in, cotan_in, lambdas, QBLOCK
    )
    lambda_grad = lax.psum(grad_lambda, "dp")
    grad_value_local = grad_value.reshape(seq_length, head_count * 2 * head_width)
    grad_value_tokens = lax.all_to_all(
        grad_value_local[None], "sp", split_axis=1, concat_axis=2, tiled=True
    )[0]
    grad_rows = lax.dot_general(
        grad_value_tokens,
        lax.all_gather(value_weight, ("sp", "dp"), axis=0, tiled=True),
        (((1,), (1,)), ((), ())),
        preferred_element_type=jnp.float32,
    )
    grad_tokens = grad_rows.astype(jnp.bfloat16)[None]
    all_tokens = lax.all_gather(tokens, "sp", axis=1, tiled=True)[0]
    sp_count = lax.axis_size("sp")
    dp_count = lax.axis_size("dp")
    token_blocks = all_tokens.reshape(seq_length, sp_count, dp_count, row_count)
    group_rows = sp_count * row_count
    term = jnp.einsum(
        "lsdb,lf->dsbf", token_blocks, grad_value_local, preferred_element_type=jnp.float32
    )
    by_batch = lax.psum_scatter(
        term.reshape(group_rows * lax.axis_size("dp"), grad_value_local.shape[1]).astype(
            jnp.bfloat16
        ),
        "dp",
        scatter_dimension=0,
        tiled=True,
    ).astype(jnp.float32)
    grad_weight = lax.all_to_all(
        by_batch.astype(jnp.bfloat16), "sp", split_axis=0, concat_axis=1, tiled=True
    ).astype(by_batch.dtype)
    grad_query_out = grad_query.reshape(1, seq_length, head_count, 2 * head_width)
    grad_key_out = grad_key.reshape(1, seq_length, head_count, 2 * head_width)
    return (grad_query_out, grad_key_out, grad_tokens, grad_weight, lambda_grad)


def solution(mesh):
    placed = (
        P("dp", "sp", None),
        P("dp", "sp", None),
        P(("sp", "dp"), None),
        P("dp", None, "sp", None),
        P("dp", None, "sp", None),
        P("sp"),
    )
    return jax.shard_map(
        body,
        mesh=mesh,
        in_specs=placed,
        out_specs=(
            P("dp", None, "sp", None),
            P("dp", None, "sp", None),
            P("dp", "sp", None),
            P(("sp", "dp"), None),
            P("sp"),
        ),
        check_vma=False,
    )
```

profile of v0, /device:TPU:0, one launch (start us, length us, event | category | flops | bytes accessed | tf_op | source)
XLA Modules:
  0.0 284.3 jit_solution(9939884770805880808)
XLA Ops:
  7.9 2.4 copy.205
  10.8 11.5 %reduce.16 = bf16[2048,128]{1,0:T(8,128)(2,1)S(1)} reduce(bf16[2048,1,128]{2,1,0:T(2,128)(2,1)S(1)} %bitcast.324, bf16[]{:T(256)} %broadcast.337), dimensions={1}, to_apply=%bitcast.242.reduce_sub_computation | reduce | bytes 1048578
  23.2 7.4 %all-to-all-start.1 = ((bf16[8,2,16384]{2,1,0:T(2,128)(2,1)}), bf16[8,2,16384]{2,1,0:T(2,128)(2,1)}, u32[]{:S(2)}, u32[]{:S(2)}) async-start(bf16[8,2,16384]{2,1,0:T(2,128)(2,1)} %reshape.398), calls=%async_computation.1 | async-start | bytes 1048576 | tf_op jit(solution)/shard_map/all_to_all | solution.py:98
  40.5 2.9 %fusion.156 = (f32[2,2,256]{2,1,0:T(2,128)S(1)}, f32[2,2,256,768]{3,2,1,0:T(8,128)}) fusion(pred[256,768]{1,0:T(8,128)(4,1)S(1)} %copy-done.51, bf16[256,2,2,64]{0,3,2,1:T(8,128)(2,1)S(1)} %bitcast.339, bf16[768,2,2,64]{0,3,2,1:T(8,128)(2,1)S(1)} %bitcast.348), kind=kOutput, calls=%fused_computation.203 | convolution fusion | flops 103809792 | bytes 3870720 | tf_op jit(solution)/shard_map/sub | solution.py:41
  43.4 2.2 broadcast_divide_fusion.1
  45.6 4.7 %fusion.155 = (f32[2,2,256]{2,1,0:T(2,128)S(1)}, f32[2,2,256,1024]{3,2,1,0:T(8,128)}) fusion(pred[256,1024]{1,0:T(8,128)(4,1)} %iota_compare_fusion, bf16[256,2,2,64]{0,3,2,1:T(8,128)(2,1)S(1)} %bitcast.335, bf16[1024,2,2,64]{0,3,2,1:T(8,128)(2,1)} %bitcast.343), kind=kOutput, calls=%fused_computation.202 | convolution fusion | flops 138413056 | bytes 5115904 | tf_op jit(solution)/shard_map/sub | solution.py:41
  50.3 4.8 %broadcast_divide_fusion = f32[2,2,256,1024]{3,2,1,0:T(8,128)} fusion(f32[2,2,256,1024]{3,2,1,0:T(8,128)} %get-tuple-element.153, f32[2,2,256]{2,1,0:T(2,128)S(1)} %get-tuple-element.152), kind=kLoop, calls=%fused_computation.38 | loop fusion | flops 1048576 | bytes 8392704 | tf_op jit(solution)/shard_map/div | solution.py:42
  55.1 1.5 fusion.158
  56.6 2.3 broadcast_divide_fusion.3
  58.9 34.5 %all-gather.3.cloned.1.call-done = bf16[2048,2048]{1,0:T(8,128)(2,1)} async-done(((bf16[64,2048]{1,0:T(8,128)(2,1)}), bf16[2048,2048]{1,0:T(8,128)(2,1)}) %all-gather.3.cloned.1.call-update) | async-done | bytes 8388624 | tf_op jit(solution)/shard_map/all_gather | solution.py:93
  93.4 5.6 %fusion.18 = bf16[1,128,2048]{2,1,0:T(8,128)(2,1)} fusion(bf16[2048,2048]{1,0:T(8,128)(2,1)} %all-gather.3.cloned.1.call-done, bf16[1,128,2048]{2,1,0:T(8,128)(2,1)} %param.26), kind=kOutput, calls=%fused_computation.26 | convolution fusion | flops 1074003968 | bytes 9437184 | tf_op jit(solution)/shard_map/dot_general | solution.py:91
  99.0 3.6 %copy.202 = bf16[1,128,2048]{1,0,2:T(2,128)(2,1)} copy(bf16[1,128,2048]{2,1,0:T(8,128)(2,1)} %fusion.18) | data formatting | bytes 1048576 | tf_op jit(solution)/shard_map/broadcast_in_dim | solution.py:96
  102.6 13.9 %reduce.17 = bf16[2048,128]{1,0:T(8,128)(2,1)} reduce(bf16[2048,1,128]{2,1,0:T(2,128)(2,1)} %bitcast.326, bf16[]{:T(256)} %broadcast.337), dimensions={1}, to_apply=%bitcast.244.reduce_sub_computation | reduce | bytes 1048578
  116.5 2.0 reshape.400
  118.4 4.1 %all-to-all-start = ((bf16[8,2,16384]{2,1,0:T(2,128)(2,1)}), bf16[8,2,16384]{2,1,0:T(2,128)(2,1)}, u32[]{:S(2)}, u32[]{:S(2)}) async-start(bf16[8,2,16384]{2,1,0:T(2,128)(2,1)} %reshape.400), calls=%async_computation | async-start | bytes 1048576 | tf_op jit(solution)/shard_map/all_to_all | solution.py:99
  122.6 2.2 subtract_convert_fusion.3
  126.0 1.6 subtract_convert_fusion
  127.6 3.7 %reshape.399 = bf16[2048,1,128]{2,1,0:T(2,128)(2,1)} reshape(bf16[8,2,16384]{2,1,0:T(2,128)(2,1)} %all-to-all-done.1) | data formatting | bytes 1048576
  140.9 6.0 %all-to-all-done = bf16[8,2,16384]{2,1,0:T(2,128)(2,1)} async-done(((bf16[8,2,16384]{2,1,0:T(2,128)(2,1)}), bf16[8,2,16384]{2,1,0:T(2,128)(2,1)}, u32[]{:S(2)}, u32[]{:S(2)}) %all-to-all-start) | async-done | bytes 524320 | tf_op jit(solution)/shard_map/all_to_all | solution.py:99
  146.9 3.5 %reshape.401 = bf16[2048,1,128]{2,1,0:T(2,128)(2,1)} reshape(bf16[8,2,16384]{2,1,0:T(2,128)(2,1)} %all-to-all-done) | data formatting | bytes 1048576
  157.3 2.1 reshape_squeeze.12
  159.4 1.9 copy.223
  161.3 1.9 slice.340
  165.4 1.6 multiply_convert_fusion.3
  167.0 2.5 fusion.79
  169.5 2.6 fusion.82
  181.9 3.1 %fusion.54 = f32[2,1,256,512]{3,2,0,1:T(8,128)} fusion(f32[2,2,256,512]{3,2,1,0:T(8,128)} %copy-done.1, bf16[256,2,128]{0,2,1:T(8,128)(2,1)S(1)} %multiply_convert_fusion.2, bf16[512,2,128]{0,2,1:T(8,128)(2,1)S(1)} %slice.331), kind=kOutput, calls=%fused_computation.71 | convolution fusion | flops 135005184 | bytes 3932160 | tf_op jit(solution)/shard_map/sub | solution.py:62
  185.0 3.0 %fusion.57 = f32[2,1,256,512]{3,2,0,1:T(8,128)} fusion(f32[2,2,256,512]{3,2,1,0:T(8,128)} %copy-done.1, f32[2]{0:T(128)S(1)} %neg.3, bf16[256,2,128]{0,2,1:T(8,128)(2,1)S(1)} %multiply_convert_fusion.2, bf16[512,2,128]{0,2,1:T(8,128)(2,1)S(1)} %slice.331), kind=kOutput, calls=%fused_computation.74 | convolution fusion | flops 135267328 | bytes 3932672 | tf_op jit(solution)/shard_map/sub | solution.py:67
  189.8 1.6 fusion.115
  191.5 1.5 multiply_bitcast_fusion.3
  196.7 3.7 %fusion = f32[2,256,1024]{2,1,0:T(8,128)} fusion(f32[2,2,256,1024]{3,2,1,0:T(8,128)} %broadcast_divide_fusion, bf16[256,2,128]{0,2,1:T(8,128)(2,1)S(1)} %multiply_convert_fusion, bf16[1024,2,128]{0,2,1:T(8,128)(2,1)} %reshape_squeeze.12), kind=kOutput, calls=%fused_computation | convolution fusion | flops 134743552 | bytes 4849664 | tf_op jit(solution)/shard_map/sub | solution.py:67
  200.4 4.1 %fusion.13 = f32[256,2048]{0,1:S(1)} fusion(bf16[1024,256]{0,1:T(8,128)(2,1)} %bitcast.332, bf16[1,1024,2048]{2,1,0:T(8,128)(2,1)} %all-gather.5.cloned.1.call-done), kind=kOutput, calls=%fused_computation.14 | convolution fusion | flops 1073741824 | bytes 6815744
  205.8 3.7 %copy.243 = bf16[1,1024,256]{2,0,1:T(2,128)(2,1)} copy(bf16[1,1024,256]{1,2,0:T(8,128)(2,1)} %bitcast.333) | data formatting | bytes 1048576 | tf_op jit(solution)/shard_map/broadcast_in_dim;reshape | solution.py:114
  209.5 5.6 %reduce.18 = bf16[1024,256]{1,0:T(8,128)(2,1)} reduce(bf16[1024,1,256]{2,1,0:T(2,128)(2,1)} %bitcast.325, bf16[]{:T(256)} %broadcast.337), dimensions={1}, to_apply=%bitcast.246.reduce_sub_computation | reduce | bytes 1048578
  215.1 2.0 reshape.402
  217.1 4.8 %fusion.150 = (f32[2]{0:T(128)S(1)}, f32[2,1,256,1024]{3,2,0,1:T(8,128)}) fusion(f32[2,2,256,1024]{3,2,1,0:T(8,128)} %broadcast_divide_fusion, f32[2,256,1024]{2,1,0:T(8,128)} %fusion, f32[2]{0:T(128)S(1)} %neg.3, bf16[256,2,128]{0,2,1:T(8,128)(2,1)S(1)} %multiply_convert_fusion, bf16[1024,2,128]{0,2,1:T(8,128)(2,1)} %reshape_squeeze.12), kind=kOutput, calls=%fused_computation.198 | convolution fusion | flops 136839168 | bytes 6946832 | tf_op jit(solution)/shard_map/qhd,khd->hqk/dot_general | solution.py:53
  222.4 7.6 %all-to-all-start.2 = ((bf16[8,2,16384]{2,1,0:T(2,128)(2,1)}), bf16[8,2,16384]{2,1,0:T(2,128)(2,1)}, u32[]{:S(2)}, u32[]{:S(2)}) async-start(bf16[8,2,16384]{2,1,0:T(2,128)(2,1)} %reshape.402), calls=%async_computation.2 | async-start | bytes 1048576 | tf_op jit(solution)/shard_map/all_to_all | solution.py:113
  230.0 6.3 %psum.7 = f32[2]{0:T(128)} all-reduce(f32[2]{0:T(128)} %subtract_subtract_fusion), channel_id=1, replica_groups=mesh['sp'=8,'dp'=4] {'dp'}, use_global_device_ids=true, to_apply=%region_29.30 | all-reduce | flops 2 | bytes 16 | tf_op jit(solution)/shard_map/psum | solution.py:111
  236.3 2.8 fusion.95
  241.8 4.5 %multiply_bitcast_fusion.1 = f32[2,1,256,1024]{3,2,0,1:T(8,128)} fusion(f32[2,2,256,1024]{3,2,1,0:T(8,128)} %broadcast_divide_fusion, bf16[256,2,128]{0,2,1:T(8,128)(2,1)S(1)} %multiply_convert_fusion, bf16[1024,2,128]{0,2,1:T(8,128)(2,1)S(1)} %copy-done.4), kind=kOutput, calls=%fused_computation.34 | convolution fusion | flops 270009856 | bytes 7602176 | tf_op jit(solution)/shard_map/sub | solution.py:62
  246.3 2.4 fusion.92
  249.6 2.0 copy.249
  251.7 2.0 fusion.76
  257.1 2.0 copy.250
  259.1 2.2 reshape.403
  261.7 6.4 %all-to-all-start.3 = ((bf16[8,64,256]{2,1,0:T(8,128)(2,1)}), bf16[8,64,256]{2,1,0:T(8,128)(2,1)S(1)}, u32[]{:S(2)}, u32[]{:S(2)}) async-start(bf16[8,64,256]{2,1,0:T(8,128)(2,1)} %bitcast.352), calls=%async_computation.4 | async-start | bytes 524288 | tf_op jit(solution)/shard_map/all_to_all | solution.py:139
  268.1 7.1 %fusion.19 = bf16[1,128,2048]{2,1,0:T(8,128)(2,1)} fusion(bf16[128,2048]{0,1:T(8,128)(2,1)S(1)} %bitcast.328, bf16[2048,2048]{1,0:T(8,128)(2,1)} %all-gather.3.cloned.1.call-done), kind=kOutput, calls=%fused_computation.27 | convolution fusion | flops 1074003968 | bytes 9437184 | tf_op jit(solution)/shard_map/dot_general | solution.py:116
  275.2 1.4 all-to-all-done.3
  (214 shorter events, 57.0 us)
Async XLA Ops:
  7.2 86.2 %all-gather.3.cloned.1.call-start = ((), (), s32[]{:S(2)}) async-start(), calls=%async_computation.5 | async-start | bytes 8650752 | tf_op jit(solution)/shard_map/all_gather | solution.py:93
  22.3 9.8 %copy-start.26 = (bf16[1,1024,2,128]{3,2,1,0:T(2,128)(2,1)S(1)}, bf16[1,1024,2,128]{3,2,1,0:T(2,128)(2,1)}, u32[]{:S(2)}) copy-start(bf16[1,1024,2,128]{3,2,1,0:T(2,128)(2,1)} %param.30) | copy-start | bytes 1572868
  23.2 10.1 %slice-start = ((bf16[1,1024,2,128]{3,2,1,0:T(2,128)(2,1)}), bf16[1,256,2,128]{3,2,1,0:T(2,128)(2,1)S(1)}, s32[]{:S(2)}) async-start(bf16[1,1024,2,128]{3,2,1,0:T(2,128)(2,1)} %param.30), calls=%async_computation.8 | async-start | bytes 262144 | tf_op jit(solution)/shard_map/slice | solution.py:29
  23.2 95.2 %all-to-all-start.1 = ((bf16[8,2,16384]{2,1,0:T(2,128)(2,1)}), bf16[8,2,16384]{2,1,0:T(2,128)(2,1)}, u32[]{:S(2)}, u32[]{:S(2)}) async-start(bf16[8,2,16384]{2,1,0:T(2,128)(2,1)} %reshape.398), calls=%async_computation.1 | async-start | bytes 1048576 | tf_op jit(solution)/shard_map/all_to_all | solution.py:98
  30.7 4.6 %slice-start.1 = ((bf16[1,1024,2,128]{3,2,1,0:T(2,128)(2,1)}), bf16[1,512,2,128]{3,2,1,0:T(2,128)(2,1)S(1)}, s32[]{:S(2)}) async-start(bf16[1,1024,2,128]{3,2,1,0:T(2,128)(2,1)} %param.30), calls=%async_computation.9 | async-start | bytes 524288 | tf_op jit(solution)/shard_map/slice | solution.py:29
  30.7 169.7 %all-gather.5.cloned.1.call-start = ((), (), s32[]{:S(2)}) async-start(), calls=%async_computation.6 | async-start | bytes 4718592 | tf_op jit(solution)/shard_map/all_gather | solution.py:123
  31.4 4.0 %slice-start.2 = ((bf16[1,1024,2,128]{3,2,1,0:T(2,128)(2,1)}), bf16[1,768,2,128]{3,2,1,0:T(2,128)(2,1)S(1)}, s32[]{:S(2)}) async-start(bf16[1,1024,2,128]{3,2,1,0:T(2,128)(2,1)} %param.30), calls=%async_computation.10 | async-start | bytes 786432 | tf_op jit(solution)/shard_map/slice | solution.py:29
  32.1 3.8 %copy-start.42 = (bf16[1,1024,2,128]{3,2,1,0:T(2,128)(2,1)S(1)}, bf16[1,1024,2,128]{3,2,1,0:T(2,128)(2,1)}, u32[]{:S(2)}) copy-start(bf16[1,1024,2,128]{3,2,1,0:T(2,128)(2,1)} %param.29) | copy-start | bytes 1572868
  33.5 21.6 %copy-start.44 = (bf16[1,256,2,128]{1,3,2,0:T(8,128)(2,1)}, bf16[1,256,2,128]{1,3,2,0:T(8,128)(2,1)S(1)}, u32[]{:S(2)}) copy-start(bf16[1,256,2,128]{1,3,2,0:T(8,128)(2,1)S(1)} %copy.199) | copy-start | bytes 393220
  35.5 2.4 copy-start.49
  35.9 4.6 %copy-start.47 = (bf16[1,768,2,128]{1,3,2,0:T(8,128)(2,1)}, bf16[1,768,2,128]{1,3,2,0:T(8,128)(2,1)S(1)}, u32[]{:S(2)}) copy-start(bf16[1,768,2,128]{1,3,2,0:T(8,128)(2,1)S(1)} %copy.220) | copy-start | bytes 1179652
  36.4 18.7 %copy-start.41 = (bf16[1,256,2,128]{1,3,2,0:T(8,128)(2,1)}, bf16[1,256,2,128]{1,3,2,0:T(8,128)(2,1)S(1)}, u32[]{:S(2)}) copy-start(bf16[1,256,2,128]{1,3,2,0:T(8,128)(2,1)S(1)} %copy.198) | copy-start | bytes 393220
  36.7 8.9 %copy-start.35 = (bf16[1,256,2,128]{1,3,2,0:T(8,128)(2,1)}, bf16[1,256,2,128]{1,3,2,0:T(8,128)(2,1)S(1)}, u32[]{:S(2)}) copy-start(bf16[1,256,2,128]{1,3,2,0:T(8,128)(2,1)S(1)} %copy.229) | copy-start | bytes 393220
  36.8 3.7 %copy-start.39 = (bf16[1,256,2,128]{1,3,2,0:T(8,128)(2,1)}, bf16[1,256,2,128]{1,3,2,0:T(8,128)(2,1)S(1)}, u32[]{:S(2)}) copy-start(bf16[1,256,2,128]{1,3,2,0:T(8,128)(2,1)S(1)} %copy.219) | copy-start | bytes 393220
  50.3 4.8 %copy-start.53 = (pred[256,256]{0,1:T(8,128)(4,1)S(1)}, pred[256,256]{0,1:T(8,128)(4,1)}, u32[]{:S(2)}) copy-start(pred[256,256]{0,1:T(8,128)(4,1)} %iota_compare_fusion.3) | copy-start | bytes 196612
  118.4 28.5 %all-to-all-start = ((bf16[8,2,16384]{2,1,0:T(2,128)(2,1)}), bf16[8,2,16384]{2,1,0:T(2,128)(2,1)}, u32[]{:S(2)}, u32[]{:S(2)}) async-start(bf16[8,2,16384]{2,1,0:T(2,128)(2,1)} %reshape.400), calls=%async_computation | async-start | bytes 1048576 | tf_op jit(solution)/shard_map/all_to_all | solution.py:99
  122.6 139.1 %reduce-scatter.2.cloned.1.call-start = ((), (), s32[]{:S(2)}) async-start(), calls=%async_computation.7 | async-start | bytes 1310720 | tf_op jit(solution)/shard_map/reduce_scatter | solution.py:131
  122.6 3.4 %copy-start = (f32[2,2,256,1024]{3,2,1,0:T(8,128)S(1)}, f32[2,2,256,1024]{3,2,1,0:T(8,128)}, u32[]{:S(2)}) copy-start(f32[2,2,256,1024]{3,2,1,0:T(8,128)} %broadcast_divide_fusion) | copy-start | bytes 12582916
  172.1 3.9 %copy-start.16 = (bf16[256,2,128]{0,2,1:T(8,128)(2,1)S(1)}, bf16[256,2,128]{0,2,1:T(8,128)(2,1)}, u32[]{:S(2)}) copy-start(bf16[256,2,128]{0,2,1:T(8,128)(2,1)} %multiply_convert_fusion.3) | copy-start | bytes 393220
  172.1 3.9 %copy-start.27 = (bf16[2,256,256]{1,2,0:T(8,128)(2,1)S(1)}, bf16[2,256,256]{1,2,0:T(8,128)(2,1)}, u32[]{:S(2)}) copy-start(bf16[2,256,256]{1,2,0:T(8,128)(2,1)} %subtract_convert_fusion.3) | copy-start | bytes 786436
  173.4 3.9 %copy-start.23 = (bf16[2,256,512]{2,1,0:T(8,128)(2,1)S(1)}, bf16[2,256,512]{2,1,0:T(8,128)(2,1)}, u32[]{:S(2)}) copy-start(bf16[2,256,512]{2,1,0:T(8,128)(2,1)} %subtract_convert_fusion.2) | copy-start | bytes 1572868
  174.8 2.8 copy-start.31
  175.9 1.8 copy-start.14
  175.9 1.8 copy-start.25
  176.2 2.0 copy-start.30
  177.7 2.2 copy-start.7
  178.1 2.7 copy-start.34
  178.2 2.7 copy-start.2
  191.4 2.0 copy-start.22
  191.4 2.1 copy-start.45
  191.4 2.9 %copy-start.8 = (f32[1024,2,128]{0,2,1:T(8,128)S(1)}, f32[1024,2,128]{0,2,1:T(8,128)}, u32[]{:S(2)}) copy-start(f32[1024,2,128]{0,2,1:T(8,128)} %scatter-add.25) | copy-start | bytes 3145732
  191.4 2.9 %copy-start.24 = (bf16[2,256,512]{2,1,0:T(8,128)(2,1)S(1)}, bf16[2,256,512]{2,1,0:T(8,128)(2,1)}, u32[]{:S(2)}) copy-start(bf16[2,256,512]{2,1,0:T(8,128)(2,1)} %subtract_convert_fusion.2) | copy-start | bytes 1572868
  217.1 4.8 %copy-start.55 = (f32[2]{0:T(128)S(1)}, f32[2]{0:T(128)}, u32[]{:S(2)}) copy-start(f32[2]{0:T(128)} %fusion.123) | copy-start | bytes 28
  217.1 4.8 %copy-start.56 = (f32[2]{0:T(128)S(1)}, f32[2]{0:T(128)}, u32[]{:S(2)}) copy-start(f32[2]{0:T(128)} %fusion.134) | copy-start | bytes 28
  217.1 19.2 %copy-start.50 = (bf16[1,512,2,128]{1,3,2,0:T(8,128)(2,1)S(1)}, bf16[1,512,2,128]{1,3,2,0:T(8,128)(2,1)}, u32[]{:S(2)}) copy-start(bf16[1,512,2,128]{1,3,2,0:T(8,128)(2,1)} %copy-done.49) | copy-start | bytes 786436
  222.4 36.7 %all-to-all-start.2 = ((bf16[8,2,16384]{2,1,0:T(2,128)(2,1)}), bf16[8,2,16384]{2,1,0:T(2,128)(2,1)}, u32[]{:S(2)}, u32[]{:S(2)}) async-start(bf16[8,2,16384]{2,1,0:T(2,128)(2,1)} %reshape.402), calls=%async_computation.2 | async-start | bytes 1048576 | tf_op jit(solution)/shard_map/all_to_all | solution.py:113
  236.3 2.8 copy-start.6
  239.1 1.7 copy-start.48
  241.8 4.5 %copy-start.12 = (f32[2,1,256,1024]{3,2,0,1:T(8,128)S(1)}, f32[2,1,256,1024]{3,2,0,1:T(8,128)}, u32[]{:S(2)}) copy-start(f32[2,1,256,1024]{3,2,0,1:T(8,128)} %get-tuple-element.143) | copy-start | bytes 6291460
  241.8 4.5 %copy-start.43 = (bf16[1,1024,2,128]{1,3,2,0:T(8,128)(2,1)S(1)}, bf16[1,1024,2,128]{1,3,2,0:T(8,128)(2,1)}, u32[]{:S(2)}) copy-start(bf16[1,1024,2,128]{1,3,2,0:T(8,128)(2,1)} %copy.230) | copy-start | bytes 1572868
  246.3 2.4 copy-start.46
  246.3 2.4 copy-start.52
  248.7 2.9 %copy-start.9 = (f32[1024,2,2,64]{0,3,2,1:T(8,128)S(1)}, f32[1024,2,2,64]{0,3,2,1:T(8,128)}, u32[]{:S(2)}) copy-start(f32[1024,2,2,64]{0,3,2,1:T(8,128)} %scatter-add.20) | copy-start | bytes 3145732
  248.7 2.9 %copy-start.38 = (bf16[1,256,2,128]{1,3,2,0:T(8,128)(2,1)S(1)}, bf16[1,256,2,128]{1,3,2,0:T(8,128)(2,1)}, u32[]{:S(2)}) copy-start(bf16[1,256,2,128]{1,3,2,0:T(8,128)(2,1)} %copy-done.37) | copy-start | bytes 393220
  249.6 4.1 %copy-start.40 = (bf16[1,256,2,128]{1,3,2,0:T(8,128)(2,1)S(1)}, bf16[1,256,2,128]{1,3,2,0:T(8,128)(2,1)}, u32[]{:S(2)}) copy-start(bf16[1,256,2,128]{1,3,2,0:T(8,128)(2,1)} %copy-done.39) | copy-start | bytes 393220
  251.7 2.0 copy-start.18
  251.7 2.5 copy-start.20
  261.7 14.9 %all-to-all-start.3 = ((bf16[8,64,256]{2,1,0:T(8,128)(2,1)}), bf16[8,64,256]{2,1,0:T(8,128)(2,1)S(1)}, u32[]{:S(2)}, u32[]{:S(2)}) async-start(bf16[8,64,256]{2,1,0:T(8,128)(2,1)} %bitcast.352), calls=%async_computation.4 | async-start | bytes 524288 | tf_op jit(solution)/shard_map/all_to_all | solution.py:139
  (19 other events, 27.4 us)
Sparse Core Ops, SparseCore 0:
  10.8 82.4 all-gather.2
  95.5 76.3 all-gather.4
  205.9 27.6 reduce-scatter.1
where the time goes:
time: 290 us; the launch traced here: 284 us
  matrix products  70.5 us (24%)
  local copies, waits for them, and re-layouts  63.4 us (22%)
  other arithmetic  60.3 us (21%)
  waiting for transfers between devices  43 us (15%)
  starting transfers between devices  26 us (9%)
  between operations  14.8 us (5%)
  blocking collectives  6.28 us (2%)
    all_gather x1, waiting for transfers between devices, body(): lax.all_gather(value_weight, ('sp', 'dp'), axis=0, tiled=True)  34.5 us
    unnamed x128, local copies, waits for them, and re-layouts  31.3 us
    unnamed x4, other arithmetic  31 us
    sub x4, matrix products, head_backward(): exponent = jnp.exp(scores - highest)  10.1 us
    sub x3, matrix products, head_backward(): grad_weights - jnp.sum(grad_weights * softmaxes[:, 0], axis=-1, keepdims=...  10 us
    div x4, other arithmetic, head_backward(): softmaxes = exponent / jnp.sum(exponent, axis=-1, keepdims=True)  9.48 us
    sub x3, matrix products, head_backward(): grad_weights - jnp.sum(grad_weights * softmaxes[:, 1], axis=-1, keepdims=...  9.28 us
    dot_general x4, matrix products, head_backward(): jnp.einsum('qhd,khd->hqk', grad_mixed, values_seen, preferred_element_typ...  8.35 us
  transfers between devices with their start and end apart: 7, of which 3 were waited for; matrix products, arithmetic and copies ran while one was open for 64% of the time, Pallas kernels for 0%

commit v1 on v0

v1 whole, which is shorter than its diff:
```python
import jax
import jax.numpy as jnp
from jax import lax
from jax.experimental import pallas as pl
from jax.experimental.pallas import tpu as pltpu
from jax.sharding import Mesh
from jax.sharding import PartitionSpec as P

QBLOCK = 256


EPS = 1e-06
NEGATIVE = -1e30

NT = (((1,), (1,)), ((), ()))


def dot(a, b):
    return jnp.dot(a, b, preferred_element_type=jnp.float32)


def dot_nt(a, b):
    return lax.dot_general(a, b, NT, preferred_element_type=jnp.float32)


def attention_kernel(
    lambda_ref, q_ref, k_ref, v_ref, g_ref, gq_ref, gk_ref, gv_ref, gl_ref, dk_acc, dv_acc
):
    seq_length, width = q_ref.shape
    half = width // 2
    scaling = half ** (-0.5)
    rows = min(QBLOCK, seq_length)
    blocks = seq_length // rows
    lam = lambda_ref[pl.program_id(0)]
    first = lax.broadcasted_iota(jnp.int32, (rows, width), 1) < half
    allowed = lax.broadcasted_iota(jnp.int32, (rows, rows), 0) >= lax.broadcasted_iota(
        jnp.int32, (rows, rows), 1
    )
    grad_lambda = jnp.zeros((rows, 1), jnp.float32)

    def softmax(scores, lo):
        diagonal = jnp.where(allowed, scores[:, lo:], NEGATIVE)
        scores = jnp.concatenate([scores[:, :lo], diagonal], axis=1) if lo else diagonal
        exponent = jnp.exp(scores - jnp.max(scores, axis=-1, keepdims=True))
        return exponent * (1.0 / jnp.sum(exponent, axis=-1, keepdims=True))

    for block in reversed(range(blocks)):
        lo = block * rows
        hi = lo + rows
        q = q_ref[lo:hi, :].astype(jnp.float32) * scaling
        zero = jnp.zeros_like(q)
        stacked = jnp.concatenate([jnp.where(first, q, zero), jnp.where(first, zero, q)], axis=0)
        keys = k_ref[:hi, :]
        values = v_ref[:hi, :]
        scores = dot_nt(stacked.astype(jnp.bfloat16), keys)
        p1 = softmax(scores[:rows], lo)
        p2 = softmax(scores[rows:], lo)
        w2 = lam * p2
        weights = (p1 - w2).astype(jnp.bfloat16)
        mixed = dot(weights, values)
        inverse = lax.rsqrt(jnp.mean(mixed * mixed, axis=-1, keepdims=True) + EPS)
        normed = mixed * inverse
        cotan = g_ref[lo:hi, :].astype(jnp.float32)
        grad_mixed = inverse * (cotan - normed * jnp.mean(cotan * normed, axis=-1, keepdims=True))
        grad_weights = dot_nt(grad_mixed.astype(jnp.bfloat16), values)
        value_part = dot(grad_mixed.T.astype(jnp.bfloat16), weights)
        t1 = jnp.sum(grad_weights * p1, axis=-1, keepdims=True)
        t2 = jnp.sum(grad_weights * p2, axis=-1, keepdims=True)
        grad_lambda = grad_lambda - t2
        ds = jnp.concatenate(
            [
                (p1 * (grad_weights - t1)).astype(jnp.bfloat16),
                (w2 * (t2 - grad_weights)).astype(jnp.bfloat16),
            ],
            axis=0,
        )
        dq = dot(ds, keys)
        gq_ref[lo:hi, :] = (jnp.where(first, dq[:rows], dq[rows:]) * scaling).astype(jnp.bfloat16)
        key_part = dot(stacked.T.astype(jnp.bfloat16), ds)
        if block == blocks - 1:
            dv_acc[...] = value_part
            dk_acc[...] = key_part
        else:
            dv_acc[:, :hi] += value_part
            dk_acc[:, :hi] += key_part
    gk_ref[...] = dk_acc[...].T.astype(jnp.bfloat16)
    gv_ref[...] = dv_acc[...].T.astype(jnp.bfloat16)
    gl_ref[...] = jnp.broadcast_to(jnp.sum(grad_lambda).reshape(1, 1, 1), gl_ref.shape)


def head_backward(queries, keys, values, cotangent, lambdas):
    seq_length = queries.shape[0]
    heads = lambdas.shape[0]
    width = queries.shape[1] // heads
    block = pl.BlockSpec((seq_length, width), lambda h: (0, h))
    grads = jax.ShapeDtypeStruct(queries.shape, jnp.bfloat16)
    gq, gk, gv, gl = pl.pallas_call(
        attention_kernel,
        grid=(heads,),
        in_specs=[pl.BlockSpec(memory_space=pltpu.SMEM), block, block, block, block],
        out_specs=[block, block, block, pl.BlockSpec((1, 8, 128), lambda h: (h, 0, 0))],
        out_shape=[grads, grads, grads, jax.ShapeDtypeStruct((heads, 8, 128), jnp.float32)],
        scratch_shapes=[
            pltpu.VMEM((width, seq_length), jnp.float32),
            pltpu.VMEM((width, seq_length), jnp.float32),
        ],
        compiler_params=pltpu.CompilerParams(dimension_semantics=("arbitrary",)),
        cost_estimate=pl.CostEstimate(
            flops=20 * heads * seq_length * seq_length * width,
            bytes_accessed=14 * heads * seq_length * width,
            transcendentals=2 * heads * seq_length * seq_length,
        ),
    )(lambdas, queries, keys, values, cotangent)
    return gq, gk, gv, gl[:, 0, 0]


def partners(size):
    if size & (size - 1) == 0:
        return [[i ^ k for i in range(size)] for k in range(1, size)]
    return [[(i + k) % size for i in range(size)] for k in range(1, size)]


def source_index(target, axis):
    source = [0] * len(target)
    for sender, receiver in enumerate(target):
        source[receiver] = sender
    return jnp.array(source, jnp.int32)[lax.axis_index(axis)]


def send(x, axis, target):
    return lax.ppermute(x, axis, list(enumerate(target)))


def gathered(x, axis):
    pieces = [(lax.axis_index(axis), x)]
    for target in partners(lax.axis_size(axis)):
        pieces.append((source_index(target, axis), send(x, axis, target)))
    return pieces


def scattered_sum(x, axis):
    mine = lax.axis_index(axis)
    total = lax.dynamic_index_in_dim(x, mine, 0, keepdims=False).astype(jnp.float32)
    for target in partners(lax.axis_size(axis)):
        block = lax.dynamic_index_in_dim(
            x, jnp.array(target, jnp.int32)[mine], 0, keepdims=False
        )
        total = total + send(block, axis, target).astype(jnp.float32)
    return total


def body(tokens, cotangent, value_weight, query_heads, key_heads, lambdas):
    groups = lax.axis_size("g")
    pair = lax.axis_size("p")
    chips = lax.axis_size("x")
    cores = lax.axis_size("c")
    dp_count = chips * cores
    local_tokens = tokens[0]
    block_tokens, model_width = local_tokens.shape
    row_count, features = value_weight.shape
    head_features = features // (pair * groups)
    group_features = pair * head_features
    seq_length = query_heads.shape[1]

    some_tokens = jnp.zeros((groups, block_tokens, model_width), tokens.dtype)
    for index, piece in gathered(local_tokens, "g"):
        some_tokens = lax.dynamic_update_slice(some_tokens, piece[None], (index, 0, 0))
    some_tokens = some_tokens.reshape(groups * block_tokens, model_width)

    mine = lax.all_to_all(
        value_weight.reshape(row_count, pair, groups, head_features)
        .transpose(2, 0, 1, 3)
        .reshape(groups, row_count, group_features),
        "g",
        split_axis=0,
        concat_axis=0,
        tiled=True,
    )
    columns = jnp.zeros((pair, groups, chips, cores, row_count, group_features), mine.dtype)
    for p_index, p_piece in gathered(mine, "p"):
        for x_index, x_piece in gathered(p_piece, "x"):
            for c_index, piece in gathered(x_piece, "c"):
                columns = lax.dynamic_update_slice(
                    columns, piece[None, :, None, None], (p_index, 0, x_index, c_index, 0, 0)
                )
    columns = columns.reshape(model_width, group_features)

    cotan_heads = lax.all_to_all(
        cotangent[0], ("p", "g"), split_axis=1, concat_axis=0, tiled=True
    )
    some_values = dot(some_tokens, columns).astype(jnp.bfloat16)
    value_heads = lax.all_to_all(some_values, "p", split_axis=1, concat_axis=0, tiled=True)
    flat = (seq_length, head_features)
    gq, gk, gv, grad_lambda = head_backward(
        query_heads.reshape(flat), key_heads.reshape(flat), value_heads, cotan_heads, lambdas
    )
    lambda_grad = grad_lambda
    for x_target in [list(range(chips))] + partners(chips):
        for c_target in [list(range(cores))] + partners(cores):
            target = [x * cores + c for x in x_target for c in c_target]
            if target != list(range(dp_count)):
                lambda_grad = lambda_grad + send(grad_lambda, ("x", "c"), target)

    grad_values = lax.all_to_all(gv, "p", split_axis=0, concat_axis=1, tiled=True)

    term = lax.dot_general(
        some_tokens, grad_values, (((0,), (0,)), ((), ())), preferred_element_type=jnp.float32
    ).astype(jnp.bfloat16)
    term = term.reshape(pair, groups, chips, cores, row_count, group_features)
    term = scattered_sum(term.transpose(3, 2, 0, 1, 4, 5), "c").astype(jnp.bfloat16)
    term = scattered_sum(term, "x").astype(jnp.bfloat16)
    term = scattered_sum(term, "p").astype(jnp.bfloat16)

    parts = dot_nt(grad_values, columns).astype(jnp.bfloat16)
    parts = lax.all_to_all(
        parts.reshape(groups, block_tokens, model_width), "g", split_axis=0, concat_axis=0, tiled=True
    )
    grad_tokens = jnp.sum(parts.astype(jnp.float32), axis=0).astype(jnp.bfloat16)

    grad_weight = lax.all_to_all(term, "g", split_axis=0, concat_axis=0, tiled=True)
    grad_weight = grad_weight.reshape(groups, row_count, pair, head_features)
    grad_weight = grad_weight.transpose(1, 2, 0, 3).reshape(row_count, features)
    return (
        gq.reshape(query_heads.shape),
        gk.reshape(key_heads.shape),
        grad_tokens[None],
        grad_weight.astype(jnp.float32),
        lambda_grad,
    )


def solution(mesh):
    sp_count = mesh.shape["sp"]
    dp_count = mesh.shape["dp"]
    pair = 2 if sp_count % 2 == 0 else 1
    cores = 2 if dp_count % 2 == 0 else 1
    inner = Mesh(
        mesh.devices.reshape(pair, sp_count // pair, dp_count // cores, cores),
        ("p", "g", "x", "c"),
    )
    sp = ("p", "g")
    dp = ("x", "c")
    token_spec = P(dp, sp, None)
    head_spec = P(dp, None, sp, None)
    weight_spec = P(sp + dp, None)
    return jax.shard_map(
        body,
        mesh=inner,
        in_specs=(token_spec, token_spec, weight_spec, head_spec, head_spec, P(sp)),
        out_specs=(head_spec, head_spec, token_spec, weight_spec, P(sp)),
        check_vma=False,
    )
```

time: 290 us -> 190 us (0.66); the launches traced: 284 us -> 189 us
  matrix products: 70.5 us -> 5.27 us
  other arithmetic: 60.3 us -> 3.05 us
  local copies, waits for them, and re-layouts: 63.4 us -> 19.7 us
  waiting for transfers between devices: 43 us -> 84.1 us
  Pallas kernels: 0 us -> 14 us
  starting transfers between devices: 26 us -> 35.4 us
  blocking collectives: 6.28 us -> 15.3 us
    ppermute x0 -> x16, waiting for transfers between devices: none -> 52.3 us  [send(): return lax.ppermute(x, axis, list(enumerate(target)))]
    all_gather x2 -> x0, waiting for transfers between devices: 34.5 us -> none  [the longest x1 34.5 us: body(): lax.all_gather(value_weight, ('sp', 'dp'), axis=0, tiled=True)]
    dot_general x22 -> x3, matrix products: 37.1 us -> 5.27 us  [the longest x1 2.66 us: dot_nt(): return lax.dot_general(a, b, NT, preferred_element_type=jnp.float32)]
    unnamed x4 -> x0, other arithmetic: 31 us -> none
    unnamed x128 -> x25, local copies, waits for them, and re-layouts: 31.3 us -> 0.97 us
    sub x10 -> x0, matrix products: 29.4 us -> none  [the longest x4 10.1 us: head_backward(): exponent = jnp.exp(scores - highest)]
    all_to_all x4 -> x5, waiting for transfers between devices: 7.42 us -> 31.8 us  [the longest x1 17.1 us: body(): lax.all_to_all(parts.reshape(groups, block_tokens, model_width), 'g', spl...]
    all_to_all x0 -> x1, blocking collectives: none -> 15.3 us  [body(): lax.all_to_all(gv, 'p', split_axis=0, concat_axis=1, tiled=True)]
  transfers between devices with their start and end apart: 7 -> 21, of which waited for: 3 -> 11; matrix products, arithmetic and copies ran while one was open for 64% -> 10% of each run, Pallas kernels for 0% -> 0%
where the time goes in v1:
time: 190 us; the launch traced here: 189 us
  waiting for transfers between devices  84.1 us (44%)
  starting transfers between devices  35.4 us (19%)
  local copies, waits for them, and re-layouts  19.7 us (10%)
  blocking collectives  15.3 us (8%)
  Pallas kernels  14 us (7%)
  between operations  12.3 us (6%)
  matrix products  5.27 us (3%)
  other arithmetic  3.05 us (2%)
    ppermute x16, waiting for transfers between devices, send(): return lax.ppermute(x, axis, list(enumerate(target)))  52.3 us
    all_to_all x1, waiting for transfers between devices, body(): lax.all_to_all(parts.reshape(groups, block_tokens, model_width), 'g', spl...  17.1 us
    all_to_all x1, blocking collectives, body(): lax.all_to_all(gv, 'p', split_axis=0, concat_axis=1, tiled=True)  15.3 us
    pallas_call x1, Pallas kernels, head_backward(): pl.pallas_call(attention_kernel, grid=(heads,), in_specs=[pl.BlockSpec(me...  14 us
    ppermute x16, starting transfers between devices, send(): return lax.ppermute(x, axis, list(enumerate(target)))  13.3 us
    all_to_all x1, waiting for transfers between devices, body(): lax.all_to_all(some_values, 'p', split_axis=1, concat_axis=0, tiled=True)  11.7 us
    all_to_all x1, starting transfers between devices, body(): lax.all_to_all(cotangent[0], ('p', 'g'), split_axis=1, concat_axis=0, til...  6.22 us
    all_to_all x1, starting transfers between devices, body(): lax.all_to_all(value_weight.reshape(row_count, pair, groups, head_feature...  5.28 us
  transfers between devices with their start and end apart: 21, of which 11 were waited for; matrix products, arithmetic and copies ran while one was open for 10% of the time, Pallas kernels for 0%

profile of v1, /device:TPU:0, one launch (start us, length us, event | category | flops | bytes accessed | tf_op | source)
XLA Modules:
  0.0 189.0 jit_solution(3324777502727290581)
XLA Ops:
  0.7 1.2 reshape.65
  2.1 0.9 reshape.66
  3.0 5.3 %all-to-all-start = ((bf16[4,64,512]{2,1,0:T(8,128)(2,1)}), bf16[4,64,512]{2,1,0:T(8,128)(2,1)S(1)}, u32[]{:S(2)}, u32[]{:S(2)}) async-start(bf16[4,64,512]{2,1,0:T(8,128)(2,1)} %reshape.66), calls=%async_computation | async-start | bytes 524288 | tf_op jit(solution)/shard_map/all_to_all | solution.py:170
  8.3 2.0 %collective-permute-start = (bf16[128,2048]{1,0:T(8,128)(2,1)S(1)}, bf16[128,2048]{1,0:T(8,128)(2,1)}, u32[]{:S(2)}, u32[]{:S(2)}) collective-permute-start(bf16[128,2048]{1,0:T(8,128)(2,1)S(1)} %bitcast.123), channel_id=1, source_target_pairs={{0,4},{4,0},{8,12},{12,8},{1,5},{5,1},{9,13},{13,9},{2,6},{6,2},{1... | collective-permute-start | bytes 1572872 | tf_op jit(solution)/shard_map/ppermute | solution.py:131
  10.3 1.5 collective-permute-start.1
  11.8 0.6 fusion.3
  16.1 0.6 dynamic_slice.60
  18.0 0.6 dynamic_slice.61
  19.9 0.6 dynamic_slice.62
  21.9 0.9 copy.51
  26.9 6.2 %all-to-all-start.2 = ((bf16[128,8,256]{2,0,1:T(8,128)(2,1)}), bf16[128,8,256]{2,0,1:T(8,128)(2,1)S(1)}, u32[]{:S(2)}, u32[]{:S(2)}) async-start(bf16[128,8,256]{2,0,1:T(8,128)(2,1)} %copy.51), calls=%async_computation.2 | async-start | bytes 1048576 | tf_op jit(solution)/shard_map/all_to_all | solution.py:188
  33.1 1.6 collective-permute-start.4
  34.9 2.9 %collective-permute-start.6 = (bf16[4,64,512]{2,1,0:T(8,128)(2,1)S(1)}, bf16[4,64,512]{2,1,0:T(8,128)(2,1)S(1)}, u32[]{:S(2)}, u32[]{:S(2)}) collective-permute-start(bf16[4,64,512]{2,1,0:T(8,128)(2,1)S(1)} %all-to-all-done), channel_id=1, source_target_pairs={{0,16},{16,0},{1,17},{17,1},{2,18},{18,2},{3,19},{19,3},{4,20},{20... | collective-permute-start | bytes 786440 | tf_op jit(solution)/shard_map/ppermute | solution.py:131
  37.8 1.1 bitcast_dynamic-update-slice_fusion.2
  38.9 1.1 bitcast_dynamic-update-slice_fusion.1
  40.0 0.7 collective-permute-done.2
  40.7 1.1 bitcast_dynamic-update-slice_fusion
  41.8 15.7 %collective-permute-done.6 = bf16[4,64,512]{2,1,0:T(8,128)(2,1)S(1)} collective-permute-done((bf16[4,64,512]{2,1,0:T(8,128)(2,1)S(1)}, bf16[4,64,512]{2,1,0:T(8,128)(2,1)S(1)}, u32[]{:S(2)}, u32[]{:S(2)}) %collective-permute-start.6) | collective-permute-done | bytes 262176 | tf_op jit(solution)/shard_map/ppermute | solution.py:131
  57.4 1.5 collective-permute-start.8
  59.2 6.9 %collective-permute-done.8 = bf16[4,64,512]{2,1,0:T(8,128)(2,1)S(1)} collective-permute-done((bf16[4,64,512]{2,1,0:T(8,128)(2,1)S(1)}, bf16[4,64,512]{2,1,0:T(8,128)(2,1)S(1)}, u32[]{:S(2)}, u32[]{:S(2)}) %collective-permute-start.8) | collective-permute-done | bytes 262176 | tf_op jit(solution)/shard_map/ppermute | solution.py:131
  66.3 1.4 collective-permute-done.9
  67.7 1.3 convolution_convert_fusion.2
  69.1 1.0 copy.50
  70.1 3.5 %all-to-all-start.1 = ((bf16[512,2,256]{2,0,1:T(8,128)(2,1)}), bf16[512,2,256]{2,0,1:T(8,128)(2,1)S(1)}, u32[]{:S(2)}, u32[]{:S(2)}) async-start(bf16[512,2,256]{2,0,1:T(8,128)(2,1)} %copy.50), calls=%async_computation.1 | async-start | bytes 1048576 | tf_op jit(solution)/shard_map/all_to_all | solution.py:192
  73.6 2.3 %copy_bitcast_fusion = (bf16[1024,256]{1,0:T(8,128)(2,1)}, bf16[1024,256]{1,0:T(8,128)(2,1)}) fusion(bf16[128,8,2,128]{3,2,1,0:T(2,128)(2,1)} %bitcast.126, bf16[128,8,2,128]{3,2,1,0:T(2,128)(2,1)} %bitcast.127), kind=kLoop, calls=%fused_computation.8 | loop fusion | bytes 2097152 | tf_op jit(solution)/shard_map/reshape | solution.py:195
  75.9 11.7 %all-to-all-done.1 = bf16[512,2,256]{2,0,1:T(8,128)(2,1)S(1)} async-done(((bf16[512,2,256]{2,0,1:T(8,128)(2,1)}), bf16[512,2,256]{2,0,1:T(8,128)(2,1)S(1)}, u32[]{:S(2)}, u32[]{:S(2)}) %all-to-all-start.1) | async-done | bytes 524320 | tf_op jit(solution)/shard_map/all_to_all | solution.py:192
  87.6 0.8 copy-done.6
  88.4 14.0 %shard_map.218 = (bf16[1024,256]{1,0:T(8,128)(2,1)}, bf16[1024,256]{1,0:T(8,128)(2,1)}, bf16[1024,256]{1,0:T(8,128)(2,1)}, f32[2,8,128]{2,1,0:T(8,128)}) custom-call(f32[2]{0:T(128)} %lambda_ref.1, bf16[1024,256]{1,0:T(8,128)(2,1)} %get-tuple-element.17.q_ref, bf16[1024,256]{1,0:T(8,128)(2,1)} %get-tuple-element.16.k_ref, bf16[1024,256]{1,0:T(8,128)(2,1)} %bitcast.120, ...), custom_call_target="tpu_custom_call" | custom-call | flops 5368709120 | bytes 3670016 | tf_op jit(solution)/shard_map/pallas_call | solution.py:97
  102.3 1.3 copy.52
  103.6 15.3 %all_to_all.72 = bf16[2,512,256]{1,2,0:T(8,128)(2,1)S(1)} all-to-all(bf16[2,512,256]{1,2,0:T(8,128)(2,1)S(1)} %copy.52), channel_id=1, replica_groups=mesh['p'=2,'g'=4,'x'=2,'c'=2] {'p'}, dimensions={0} | all-to-all | bytes 1048576 | tf_op jit(solution)/shard_map/all_to_all | solution.py:204
  118.9 1.3 convolution_convert_fusion
  120.4 2.6 %collective-permute-done.10 = bf16[2,2,4,64,512]{4,3,0,2,1:T(8,128)(2,1)S(1)} collective-permute-done((bf16[2,2,4,64,512]{4,3,0,2,1:T(8,128)(2,1)S(1)}, bf16[2,2,4,64,512]{4,3,0,2,1:T(8,128)(2,1)S(1)}, u32[]{:S(2)}, u32[]{:S(2)}) %collective-permute-start.10) | collective-permute-done | bytes 1048608 | tf_op jit(solution)/shard_map/ppermute | solution.py:131
  123.4 1.6 collective-permute-start.11
  125.0 12.5 %collective-permute-done.11 = bf16[2,4,64,512]{3,2,1,0:T(8,128)(2,1)S(1)} collective-permute-done((bf16[2,4,64,512]{3,2,1,0:T(8,128)(2,1)S(1)}, bf16[2,4,64,512]{3,2,1,0:T(8,128)(2,1)S(1)}, u32[]{:S(2)}, u32[]{:S(2)}) %collective-permute-start.11) | collective-permute-done | bytes 524320 | tf_op jit(solution)/shard_map/ppermute | solution.py:131
  137.7 11.6 %collective-permute-done.12 = bf16[4,64,512]{2,1,0:T(8,128)(2,1)S(1)} collective-permute-done((bf16[4,64,512]{2,1,0:T(8,128)(2,1)S(1)}, bf16[4,64,512]{2,1,0:T(8,128)(2,1)S(1)}, u32[]{:S(2)}, u32[]{:S(2)}) %collective-permute-start.12) | collective-permute-done | bytes 262176 | tf_op jit(solution)/shard_map/ppermute | solution.py:131
  149.3 0.8 fusion.2
  150.1 3.4 %all-to-all-start.5 = ((bf16[4,64,512]{2,1,0:T(8,128)(2,1)}), bf16[4,64,512]{2,1,0:T(8,128)(2,1)S(1)}, u32[]{:S(2)}, u32[]{:S(2)}) async-start(bf16[4,64,512]{2,1,0:T(8,128)(2,1)} %fusion.2), calls=%async_computation.5 | async-start | bytes 524288 | tf_op jit(solution)/shard_map/all_to_all | solution.py:220
  153.5 2.7 %convolution_convert_fusion.1 = bf16[512,2048]{1,0:T(8,128)(2,1)} fusion(bf16[512,512]{0,1:T(8,128)(2,1)S(1)} %bitcast.119, bf16[2048,512]{1,0:T(8,128)(2,1)S(1)} %bitcast.111), kind=kOutput, calls=%fused_computation.1 | convolution fusion | flops 1074790400 | bytes 4718592 | tf_op jit(solution)/shard_map/dot_general | solution.py:23
  156.2 3.1 %all-to-all-done.5 = bf16[4,64,512]{2,1,0:T(8,128)(2,1)S(1)} async-done(((bf16[4,64,512]{2,1,0:T(8,128)(2,1)}), bf16[4,64,512]{2,1,0:T(8,128)(2,1)S(1)}, u32[]{:S(2)}, u32[]{:S(2)}) %all-to-all-start.5) | async-done | bytes 262176 | tf_op jit(solution)/shard_map/all_to_all | solution.py:220
  159.3 3.7 %all-to-all-start.4 = ((bf16[4,128,2048]{2,1,0:T(8,128)(2,1)}), bf16[4,128,2048]{2,1,0:T(8,128)(2,1)S(1)}, u32[]{:S(2)}, u32[]{:S(2)}) async-start(bf16[4,128,2048]{2,1,0:T(8,128)(2,1)} %bitcast.112), calls=%async_computation.4 | async-start | bytes 4194304 | tf_op jit(solution)/shard_map/all_to_all | solution.py:215
  163.1 0.8 slice_reduce_fusion
  163.9 1.6 collective-permute-start.14
  165.7 0.9 reshape.68
  166.6 0.9 reshape.69
  167.6 0.8 collective-permute-done.15
  169.6 1.1 reshape.75
  170.7 17.1 %all-to-all-done.4 = bf16[4,128,2048]{2,1,0:T(8,128)(2,1)S(1)} async-done(((bf16[4,128,2048]{2,1,0:T(8,128)(2,1)}), bf16[4,128,2048]{2,1,0:T(8,128)(2,1)S(1)}, u32[]{:S(2)}, u32[]{:S(2)}) %all-to-all-start.4) | async-done | bytes 2097184 | tf_op jit(solution)/shard_map/all_to_all | solution.py:215
  187.7 1.3 reduce_sum.12
  (63 shorter events, 3.7 us)
Async XLA Ops:
  0.6 11.2 %copy-start.8 = (s32[2]{0:T(128)S(1)}, s32[2]{0:T(128)}, u32[]{:S(2)}) copy-start(s32[2]{0:T(128)} %constant.55.clone) | copy-start | bytes 28
  0.6 15.4 %copy-start.11 = (s32[4]{0:T(128)S(1)}, s32[4]{0:T(128)}, u32[]{:S(2)}) copy-start(s32[4]{0:T(128)} %constant.52.clone) | copy-start | bytes 52
  0.7 17.3 %copy-start.10 = (s32[4]{0:T(128)S(1)}, s32[4]{0:T(128)}, u32[]{:S(2)}) copy-start(s32[4]{0:T(128)} %constant.53.clone) | copy-start | bytes 52
  0.7 19.2 %copy-start.9 = (s32[4]{0:T(128)S(1)}, s32[4]{0:T(128)}, u32[]{:S(2)}) copy-start(s32[4]{0:T(128)} %constant.54.clone) | copy-start | bytes 52
  0.7 7.6 %copy-start.7 = (bf16[1,128,2048]{2,1,0:T(8,128)(2,1)S(1)}, bf16[1,128,2048]{2,1,0:T(8,128)(2,1)}, u32[]{:S(2)}) copy-start(bf16[1,128,2048]{2,1,0:T(8,128)(2,1)} %param.19) | copy-start | bytes 1572868
  0.7 21.1 %copy-start.2 = (bf16[1,128,2048]{2,1,0:T(8,128)(2,1)S(1)}, bf16[1,128,2048]{2,1,0:T(8,128)(2,1)}, u32[]{:S(2)}) copy-start(bf16[1,128,2048]{2,1,0:T(8,128)(2,1)} %param.20) | copy-start | bytes 1572868
  3.0 23.8 %all-to-all-start = ((bf16[4,64,512]{2,1,0:T(8,128)(2,1)}), bf16[4,64,512]{2,1,0:T(8,128)(2,1)S(1)}, u32[]{:S(2)}, u32[]{:S(2)}) async-start(bf16[4,64,512]{2,1,0:T(8,128)(2,1)} %reshape.66), calls=%async_computation | async-start | bytes 524288 | tf_op jit(solution)/shard_map/all_to_all | solution.py:170
  8.3 26.6 %collective-permute-start = (bf16[128,2048]{1,0:T(8,128)(2,1)S(1)}, bf16[128,2048]{1,0:T(8,128)(2,1)}, u32[]{:S(2)}, u32[]{:S(2)}) collective-permute-start(bf16[128,2048]{1,0:T(8,128)(2,1)S(1)} %bitcast.123), channel_id=1, source_target_pairs={{0,4},{4,0},{8,12},{12,8},{1,5},{5,1},{9,13},{13,9},{2,6},{6,2},{1... | collective-permute-start | bytes 1572872 | tf_op jit(solution)/shard_map/ppermute | solution.py:131
  10.3 28.6 %collective-permute-start.1 = (bf16[128,2048]{1,0:T(8,128)(2,1)S(1)}, bf16[128,2048]{1,0:T(8,128)(2,1)}, u32[]{:S(2)}, u32[]{:S(2)}) collective-permute-start(bf16[128,2048]{1,0:T(8,128)(2,1)S(1)} %bitcast.124), channel_id=1, source_target_pairs={{0,8},{4,12},{8,0},{12,4},{1,9},{5,13},{9,1},{13,5},{2,10},{6,14},... | collective-permute-start | bytes 1572872 | tf_op jit(solution)/shard_map/ppermute | solution.py:131
  11.8 28.9 %collective-permute-start.2 = (bf16[128,2048]{1,0:T(8,128)(2,1)S(1)}, bf16[128,2048]{1,0:T(8,128)(2,1)}, u32[]{:S(2)}, u32[]{:S(2)}) collective-permute-start(bf16[128,2048]{1,0:T(8,128)(2,1)S(1)} %bitcast.125), channel_id=1, source_target_pairs={{0,12},{4,8},{8,4},{12,0},{1,13},{5,9},{9,5},{13,1},{2,14},{6,10},... | collective-permute-start | bytes 1572872 | tf_op jit(solution)/shard_map/ppermute | solution.py:131
  26.9 43.2 %all-to-all-start.2 = ((bf16[128,8,256]{2,0,1:T(8,128)(2,1)}), bf16[128,8,256]{2,0,1:T(8,128)(2,1)S(1)}, u32[]{:S(2)}, u32[]{:S(2)}) async-start(bf16[128,8,256]{2,0,1:T(8,128)(2,1)} %copy.51), calls=%async_computation.2 | async-start | bytes 1048576 | tf_op jit(solution)/shard_map/all_to_all | solution.py:188
  33.1 26.1 %collective-permute-start.3 = (bf16[4,64,512]{2,1,0:T(8,128)(2,1)S(1)}, bf16[4,64,512]{2,1,0:T(8,128)(2,1)S(1)}, u32[]{:S(2)}, u32[]{:S(2)}) collective-permute-start(bf16[4,64,512]{2,1,0:T(8,128)(2,1)S(1)} %all-to-all-done), channel_id=1, source_target_pairs={{0,1},{1,0},{2,3},{3,2},{4,5},{5,4},{6,7},{7,6},{8,9},{9,8},{10,11... | collective-permute-start | bytes 786440 | tf_op jit(solution)/shard_map/ppermute | solution.py:131
  33.1 25.9 %collective-permute-start.4 = (bf16[4,64,512]{2,1,0:T(8,128)(2,1)S(1)}, bf16[4,64,512]{2,1,0:T(8,128)(2,1)S(1)}, u32[]{:S(2)}, u32[]{:S(2)}) collective-permute-start(bf16[4,64,512]{2,1,0:T(8,128)(2,1)S(1)} %all-to-all-done), channel_id=1, source_target_pairs={{0,2},{2,0},{1,3},{3,1},{4,6},{6,4},{5,7},{7,5},{8,10},{10,8},{9,1... | collective-permute-start | bytes 786440 | tf_op jit(solution)/shard_map/ppermute | solution.py:131
  34.9 22.5 %collective-permute-start.6 = (bf16[4,64,512]{2,1,0:T(8,128)(2,1)S(1)}, bf16[4,64,512]{2,1,0:T(8,128)(2,1)S(1)}, u32[]{:S(2)}, u32[]{:S(2)}) collective-permute-start(bf16[4,64,512]{2,1,0:T(8,128)(2,1)S(1)} %all-to-all-done), channel_id=1, source_target_pairs={{0,16},{16,0},{1,17},{17,1},{2,18},{18,2},{3,19},{19,3},{4,20},{20... | collective-permute-start | bytes 786440 | tf_op jit(solution)/shard_map/ppermute | solution.py:131
  57.4 8.8 %collective-permute-start.7 = (bf16[4,64,512]{2,1,0:T(8,128)(2,1)S(1)}, bf16[4,64,512]{2,1,0:T(8,128)(2,1)S(1)}, u32[]{:S(2)}, u32[]{:S(2)}) collective-permute-start(bf16[4,64,512]{2,1,0:T(8,128)(2,1)S(1)} %collective-permute-done.6), channel_id=1, source_target_pairs={{0,1},{1,0},{2,3},{3,2},{4,5},{5,4},{6,7},{7,6},{8,9},{9,8},{10,11... | collective-permute-start | bytes 786440 | tf_op jit(solution)/shard_map/ppermute | solution.py:131
  57.4 8.7 %collective-permute-start.8 = (bf16[4,64,512]{2,1,0:T(8,128)(2,1)S(1)}, bf16[4,64,512]{2,1,0:T(8,128)(2,1)S(1)}, u32[]{:S(2)}, u32[]{:S(2)}) collective-permute-start(bf16[4,64,512]{2,1,0:T(8,128)(2,1)S(1)} %collective-permute-done.6), channel_id=1, source_target_pairs={{0,2},{2,0},{1,3},{3,1},{4,6},{6,4},{5,7},{7,5},{8,10},{10,8},{9,1... | collective-permute-start | bytes 786440 | tf_op jit(solution)/shard_map/ppermute | solution.py:131
  58.9 7.2 %collective-permute-start.5 = (bf16[4,64,512]{2,1,0:T(8,128)(2,1)S(1)}, bf16[4,64,512]{2,1,0:T(8,128)(2,1)S(1)}, u32[]{:S(2)}, u32[]{:S(2)}) collective-permute-start(bf16[4,64,512]{2,1,0:T(8,128)(2,1)S(1)} %collective-permute-done.4), channel_id=1, source_target_pairs={{0,1},{1,0},{2,3},{3,2},{4,5},{5,4},{6,7},{7,6},{8,9},{9,8},{10,11... | collective-permute-start | bytes 786440 | tf_op jit(solution)/shard_map/ppermute | solution.py:131
  66.2 1.5 collective-permute-start.9
  67.7 1.3 copy-start
  70.1 17.5 %copy-start.3 = (bf16[128,8,256]{2,0,1:T(8,128)(2,1)}, bf16[128,8,256]{2,0,1:T(8,128)(2,1)S(1)}, u32[]{:S(2)}) copy-start(bf16[128,8,256]{2,0,1:T(8,128)(2,1)S(1)} %all-to-all-done.2) | copy-start | bytes 1572868
  70.1 17.5 %all-to-all-start.1 = ((bf16[512,2,256]{2,0,1:T(8,128)(2,1)}), bf16[512,2,256]{2,0,1:T(8,128)(2,1)S(1)}, u32[]{:S(2)}, u32[]{:S(2)}) async-start(bf16[512,2,256]{2,0,1:T(8,128)(2,1)} %copy.50), calls=%async_computation.1 | async-start | bytes 1048576 | tf_op jit(solution)/shard_map/all_to_all | solution.py:192
  87.6 0.8 copy-start.6
  120.3 2.7 %collective-permute-start.10 = (bf16[2,2,4,64,512]{4,3,0,2,1:T(8,128)(2,1)S(1)}, bf16[2,2,4,64,512]{4,3,0,2,1:T(8,128)(2,1)S(1)}, u32[]{:S(2)}, u32[]{:S(2)}) collective-permute-start(bf16[2,2,4,64,512]{4,3,0,2,1:T(8,128)(2,1)S(1)} %dynamic-slice_bitcast_fusion), channel_id=1, source_target_pairs={{0,1},{1,0},{2,3},{3,2},{4,5},{5,4},{6,7},{7,6},{8,9},{9,8},{10,11... | collective-permute-start | bytes 3145736 | tf_op jit(solution)/shard_map/ppermute | solution.py:131
  123.3 30.2 %copy-start.1 = (bf16[2,4,2,2,64,512]{5,4,3,2,1,0:T(8,128)(2,1)S(1)}, bf16[2,4,2,2,64,512]{5,4,3,2,1,0:T(8,128)(2,1)}, u32[]{:S(2)}) copy-start(bf16[2,4,2,2,64,512]{5,4,3,2,1,0:T(8,128)(2,1)} %copy-done) | copy-start | bytes 6291460
  123.4 14.0 %collective-permute-start.11 = (bf16[2,4,64,512]{3,2,1,0:T(8,128)(2,1)S(1)}, bf16[2,4,64,512]{3,2,1,0:T(8,128)(2,1)S(1)}, u32[]{:S(2)}, u32[]{:S(2)}) collective-permute-start(bf16[2,4,64,512]{3,2,1,0:T(8,128)(2,1)S(1)} %dynamic-slice_bitcast_fusion.1), channel_id=1, source_target_pairs={{0,2},{2,0},{1,3},{3,1},{4,6},{6,4},{5,7},{7,5},{8,10},{10,8},{9,1... | collective-permute-start | bytes 1572872 | tf_op jit(solution)/shard_map/ppermute | solution.py:131
  137.6 11.7 %collective-permute-start.12 = (bf16[4,64,512]{2,1,0:T(8,128)(2,1)S(1)}, bf16[4,64,512]{2,1,0:T(8,128)(2,1)S(1)}, u32[]{:S(2)}, u32[]{:S(2)}) collective-permute-start(bf16[4,64,512]{2,1,0:T(8,128)(2,1)S(1)} %dynamic-slice_bitcast_fusion.2), channel_id=1, source_target_pairs={{0,16},{16,0},{1,17},{17,1},{2,18},{18,2},{3,19},{19,3},{4,20},{20... | collective-permute-start | bytes 786440 | tf_op jit(solution)/shard_map/ppermute | solution.py:131
  150.1 9.2 %all-to-all-start.5 = ((bf16[4,64,512]{2,1,0:T(8,128)(2,1)}), bf16[4,64,512]{2,1,0:T(8,128)(2,1)S(1)}, u32[]{:S(2)}, u32[]{:S(2)}) async-start(bf16[4,64,512]{2,1,0:T(8,128)(2,1)} %fusion.2), calls=%async_computation.5 | async-start | bytes 524288 | tf_op jit(solution)/shard_map/all_to_all | solution.py:220
  159.3 6.4 %copy-start.5 = (bf16[1024,256]{1,0:T(8,128)(2,1)S(1)}, bf16[1024,256]{1,0:T(8,128)(2,1)}, u32[]{:S(2)}) copy-start(bf16[1024,256]{1,0:T(8,128)(2,1)} %get-tuple-element.9) | copy-start | bytes 1572868
  159.3 7.3 %copy-start.4 = (bf16[1024,256]{1,0:T(8,128)(2,1)S(1)}, bf16[1024,256]{1,0:T(8,128)(2,1)}, u32[]{:S(2)}) copy-start(bf16[1024,256]{1,0:T(8,128)(2,1)} %get-tuple-element.10) | copy-start | bytes 1572868
  159.3 28.4 %all-to-all-start.4 = ((bf16[4,128,2048]{2,1,0:T(8,128)(2,1)}), bf16[4,128,2048]{2,1,0:T(8,128)(2,1)S(1)}, u32[]{:S(2)}, u32[]{:S(2)}) async-start(bf16[4,128,2048]{2,1,0:T(8,128)(2,1)} %bitcast.112), calls=%async_computation.4 | async-start | bytes 4194304 | tf_op jit(solution)/shard_map/all_to_all | solution.py:215
  163.9 3.7 %collective-permute-start.13 = (f32[2]{0:T(128)S(1)}, f32[2]{0:T(128)S(1)}, u32[]{:S(2)}, u32[]{:S(2)}) collective-permute-start(f32[2]{0:T(128)S(1)} %slice_reduce_fusion), channel_id=1, source_target_pairs={{0,1},{1,0},{2,3},{3,2},{4,5},{5,4},{6,7},{7,6},{8,9},{9,8},{10,11... | collective-permute-start | bytes 32 | tf_op jit(solution)/shard_map/ppermute | solution.py:131
  163.9 3.7 %collective-permute-start.14 = (f32[2]{0:T(128)S(1)}, f32[2]{0:T(128)S(1)}, u32[]{:S(2)}, u32[]{:S(2)}) collective-permute-start(f32[2]{0:T(128)S(1)} %slice_reduce_fusion), channel_id=1, source_target_pairs={{0,2},{1,3},{2,0},{3,1},{4,6},{5,7},{6,4},{7,5},{8,10},{9,11},{10,... | collective-permute-start | bytes 32 | tf_op jit(solution)/shard_map/ppermute | solution.py:131
  165.4 3.0 %collective-permute-start.15 = (f32[2]{0:T(128)S(1)}, f32[2]{0:T(128)S(1)}, u32[]{:S(2)}, u32[]{:S(2)}) collective-permute-start(f32[2]{0:T(128)S(1)} %slice_reduce_fusion), channel_id=1, source_target_pairs={{0,3},{1,2},{2,1},{3,0},{4,7},{5,6},{6,5},{7,4},{8,11},{9,10},{10,... | collective-permute-start | bytes 32 | tf_op jit(solution)/shard_map/ppermute | solution.py:131
